TPU v7x, 32 devices: a whole 2x2x4 slice. The times are simulated.
32 devices in a mesh: grp: 2 (over y), fs: 4 (over z), tp: 4 (over x, core).
Axes of the slice: x: 2, y: 2, z: 4, core: 2. Of those that a mesh axis runs over, the one named last changes fastest.
Arguments:
- tokens: bfloat16 [4096, 2048], P(('grp', 'fs', 'tp')), parts along dimension 0, may hold values from -12 to 12
- norm_gain: float32 [2048], replicated, may hold values from 0.1 to 1.9
- w_in: bfloat16 [2048, 8192], P('fs', 'tp'), may hold values from -0.125 to 0.125
- w_out: bfloat16 [8192, 2048], P('tp', 'fs'), may hold values from -0.0625 to 0.0625
Outputs:
- mixed: bfloat16 [4096, 2048], P(('grp', 'fs', 'tp')), parts along dimension 0
There are 2 independent parts, one for each index of `grp`. A program takes and returns all parts, laid end to end along the dimension named above; an argument that names none is the same for every part. Nothing has to cross between parts.
All inputs are finite; a program needn't handle non-finite values.
Results may differ from a plain program's by a relative error of at most 0.012.
Values may be sent and summed in bfloat16 or wider, within the bound.
A program may use at most 64 MiB of HBM per device.

v0:
```python
import jax
import jax.numpy as jnp
from jax import lax
from jax.sharding import PartitionSpec as P

EPS = 1e-06


def local(tokens, norm_gain, w_in, w_out):
    xf = tokens.astype(jnp.float32)
    scale = lax.rsqrt(jnp.mean(xf * xf, axis=-1, keepdims=True) + EPS)
    normed = (xf * scale * norm_gain).astype(jnp.bfloat16)
    group = lax.all_gather(normed, "tp", axis=0, tiled=True)
    pre = jnp.dot(
        group, lax.all_gather(w_in, "fs", axis=0, tiled=True), preferred_element_type=jnp.float32
    )
    hidden = jnp.square(jax.nn.relu(pre)).astype(jnp.bfloat16)
    terms = jnp.dot(
        hidden, lax.all_gather(w_out, "fs", axis=1, tiled=True), preferred_element_type=jnp.float32
    )
    summed = lax.psum_scatter(
        terms.astype(jnp.bfloat16), "tp", scatter_dimension=0, tiled=True
    ).astype(jnp.float32)
    return (xf + summed).astype(jnp.bfloat16)


def solution(mesh):
    in_specs = (P(("grp", "fs", "tp"), None), P(), P("fs", "tp"), P("tp", "fs"))
    out_specs = P(("grp", "fs", "tp"), None)
    return jax.shard_map(local, mesh=mesh, in_specs=in_specs, out_specs=out_specs, check_vma=False)
```

profile of v0, /device:TPU:0, one launch (start us, length us, event | category | flops | bytes accessed | tf_op | source)
XLA Modules:
  0.0 390.5 jit_solution(15908731586754024758)
XLA Ops:
  6.5 0.0 all-gather.4.cloned.1.call-start
  6.5 1.2 fusion
  7.8 2.0 fusion.2
  9.8 0.0 all-gather.4.cloned.1.call-update
  9.8 0.0 all-gather.6.cloned.1.call-start
  9.9 0.7 all-gather.6.cloned.1.call-update
  10.6 0.0 all-gather.8.cloned.1.call-start
  10.6 0.7 all-gather.8.cloned.1.call-update
  11.3 0.0 copy-start
  11.3 0.0 reduce-scatter.2.cloned.1.call-start
  11.4 23.9 %all-gather.4.cloned.1.call-done = bf16[512,2048]{1,0:T(8,128)(2,1)} async-done(((bf16[128,2048]{1,0:T(8,128)(2,1)}), bf16[512,2048]{1,0:T(8,128)(2,1)}) %all-gather.4.cloned.1.call-update) | async-done | bytes 2097168 | tf_op jit(solution)/shard_map/all_gather | solution.py:13
  35.3 151.2 %all-gather.6.cloned.1.call-done = bf16[2048,2048]{1,0:T(8,128)(2,1)} async-done(((bf16[512,2048]{1,0:T(8,128)(2,1)}), bf16[2048,2048]{1,0:T(8,128)(2,1)}) %all-gather.6.cloned.1.call-update) | async-done | bytes 8388624 | tf_op jit(solution)/shard_map/all_gather | solution.py:15
  186.5 149.4 %all-gather.8.cloned.1.call-done = bf16[2048,2048]{1,0:T(8,128)(2,1)} async-done(((bf16[2048,512]{1,0:T(8,128)(2,1)}), bf16[2048,2048]{1,0:T(8,128)(2,1)}) %all-gather.8.cloned.1.call-update) | async-done | bytes 8388624 | tf_op jit(solution)/shard_map/all_gather | solution.py:19
  335.9 16.5 %convolution_convert_fusion = bf16[512,2048]{1,0:T(8,128)(2,1)} fusion(bf16[2048,2048]{1,0:T(8,128)(2,1)} %all-gather.8.cloned.1.call-done, bf16[512,2048]{1,0:T(8,128)(2,1)} %all-gather.4.cloned.1.call-done, bf16[2048,2048]{1,0:T(8,128)(2,1)} %all-gather.6.cloned.1.call-done), kind=kOutput, calls=%fused_computation.1 | convolution fusion | flops 8594128896 | bytes 20971520 | tf_op jit(solution)/shard_map/dot_general | solution.py:18
  352.4 0.0 reduce-scatter.2.cloned.1.call-update
  352.4 29.5 %reduce-scatter.2.cloned.1.call-done = bf16[128,2048]{1,0:T(8,128)(2,1)} async-done(((bf16[512,2048]{1,0:T(8,128)(2,1)}), bf16[128,2048]{1,0:T(8,128)(2,1)}) %reduce-scatter.2.cloned.1.call-update) | async-done | bytes 524304 | tf_op jit(solution)/shard_map/reduce_scatter | solution.py:21
  382.0 0.0 copy-done
  382.0 2.0 fusion.3
  (1 shorter events, 0.0 us)
Async XLA Ops:
  6.5 28.7 %all-gather.4.cloned.1.call-start = ((), (), s32[]{:S(2)}) async-start(), calls=%async_computation.1 | async-start | bytes 2621440 | tf_op jit(solution)/shard_map/all_gather | solution.py:13
  9.8 176.7 %all-gather.6.cloned.1.call-start = ((), (), s32[]{:S(2)}) async-start(), calls=%async_computation.2 | async-start | bytes 10485760 | tf_op jit(solution)/shard_map/all_gather | solution.py:15
  10.6 325.3 %all-gather.8.cloned.1.call-start = ((), (), s32[]{:S(2)}) async-start(), calls=%async_computation.3 | async-start | bytes 10485760 | tf_op jit(solution)/shard_map/all_gather | solution.py:19
  11.3 370.6 %copy-start = (bf16[128,2048]{1,0:T(8,128)(2,1)S(1)}, bf16[128,2048]{1,0:T(8,128)(2,1)}, u32[]{:S(2)}) copy-start(bf16[128,2048]{1,0:T(8,128)(2,1)} %param.4) | copy-start | bytes 1572868
  11.3 370.6 %reduce-scatter.2.cloned.1.call-start = ((), (), s32[]{:S(2)}) async-start(), calls=%async_computation.4 | async-start | bytes 2621440 | tf_op jit(solution)/shard_map/reduce_scatter | solution.py:21
Sparse Core Ops, SparseCore 0:
  9.9 25.2 all-gather.3
  36.8 149.6 all-gather.5
  188.1 147.7 all-gather.7
  352.6 29.3 reduce-scatter.1
where the time goes:
time: 391 us; the launch traced here: 390 us
  waiting for transfers between devices  355 us (91%)
  matrix products  16.5 us (4%)
  between operations  13.1 us (3%)
  other arithmetic  5.23 us (1%)
    all_gather x1, waiting for transfers between devices, local(): lax.all_gather(w_in, 'fs', axis=0, tiled=True)  151 us
    all_gather x1, waiting for transfers between devices, local(): lax.all_gather(w_out, 'fs', axis=1, tiled=True)  149 us
    reduce_scatter x1, waiting for transfers between devices, local(): lax.psum_scatter(terms.astype(jnp.bfloat16), 'tp', scatter_dimension=0, t...  29.5 us
    all_gather x1, waiting for transfers between devices, local(): group = lax.all_gather(normed, 'tp', axis=0, tiled=True)  23.9 us
    dot_general x1, matrix products, local(): jnp.dot(hidden, lax.all_gather(w_out, 'fs', axis=1, tiled=True), preferre...  16.5 us
  transfers between devices with their start and end apart: 4, of which 4 were waited for; matrix products, arithmetic and copies ran while one was open for 0% of the time, Pallas kernels for 0%

commit v1 on v0

--- a/solution.py
+++ b/solution.py
@@ -6,11 +6,21 @@
 EPS = 1e-06
 
 
+def around_the_ring(x, axis, d):
+    size = lax.axis_size(axis)
+    moving, tiles = (x, [x])
+    for _ in range(size - 1):
+        moving = lax.ppermute(moving, axis, [(i, (i + 1) % size) for i in range(size)])
+        tiles.insert(0, moving)
+    line = jnp.concatenate(tiles, axis=d)
+    return jnp.roll(line, (lax.axis_index(axis) + 1) * x.shape[d], axis=d)
+
+
 def local(tokens, norm_gain, w_in, w_out):
     xf = tokens.astype(jnp.float32)
     scale = lax.rsqrt(jnp.mean(xf * xf, axis=-1, keepdims=True) + EPS)
     normed = (xf * scale * norm_gain).astype(jnp.bfloat16)
-    group = lax.all_gather(normed, "tp", axis=0, tiled=True)
+    group = around_the_ring(normed, "tp", 0)
     pre = jnp.dot(
         group, lax.all_gather(w_in, "fs", axis=0, tiled=True), preferred_element_type=jnp.float32
     )

time: 391 us -> 365 us (0.934)
  waiting for transfers between devices: 355 us -> 326 us
  local copies, waits for them, and re-layouts: 0.01 us -> 5.05 us
    all_gather x1, waiting for transfers between devices: 151 us -> 119 us  [local(): lax.all_gather(w_in, 'fs', axis=0, tiled=True)]
    ppermute x0 -> x3, waiting for transfers between devices: none -> 26 us  [around_the_ring(): lax.ppermute(moving, axis, [(i, (i + 1) % size) for i in range(size)])]
    all_gather x1 -> x0, waiting for transfers between devices: 23.9 us -> none  [local(): group = lax.all_gather(normed, 'tp', axis=0, tiled=True)]
    unnamed x2 -> x10, local copies, waits for them, and re-layouts: 0.01 us -> 5.05 us
  transfers between devices with their start and end apart: 4 -> 6, of which waited for: 4 -> 6; matrix products, arithmetic and copies ran while one was open for 0% -> 2% of each run, Pallas kernels for 0% -> 0%
where the time goes in v1:
time: 365 us
  waiting for transfers between devices  326 us (89%)
  matrix products  16.5 us (5%)
  between operations  13.1 us (4%)
  local copies, waits for them, and re-layouts  5.05 us (1%)
  other arithmetic  4.3 us (1%)
    all_gather x1, waiting for transfers between devices, local(): lax.all_gather(w_out, 'fs', axis=1, tiled=True)  149 us
    all_gather x1, waiting for transfers between devices, local(): lax.all_gather(w_in, 'fs', axis=0, tiled=True)  119 us
    reduce_scatter x1, waiting for transfers between devices, local(): lax.psum_scatter(terms.astype(jnp.bfloat16), 'tp', scatter_dimension=0, t...  29.5 us
    ppermute x3, waiting for transfers between devices, around_the_ring(): lax.ppermute(moving, axis, [(i, (i + 1) % size) for i in range(size)])  26 us
    dot_general x1, matrix products, local(): jnp.dot(hidden, lax.all_gather(w_out, 'fs', axis=1, tiled=True), preferre...  16.5 us
  transfers between devices with their start and end apart: 6, of which 6 were waited for; matrix products, arithmetic and copies ran while one was open for 2% of the time, Pallas kernels for 0%

profile of v1, /device:TPU:0, one launch (start us, length us, event | category | flops | bytes accessed | tf_op | source)
XLA Modules:
  0.0 365.2 jit_solution(8632855996958187565)
XLA Ops:
  6.5 0.0 copy-start
  6.5 0.0 copy-start.1
  6.5 0.0 all-gather.3.cloned.1.call-start
  6.5 0.7 all-gather.3.cloned.1.call-update
  7.3 0.0 all-gather.5.cloned.1.call-start
  7.3 0.7 all-gather.5.cloned.1.call-update
  8.0 0.0 reduce-scatter.2.cloned.1.call-start
  8.1 0.0 copy-done
  8.1 0.2 fusion.1
  8.3 0.0 copy-done.1
  8.3 0.2 fusion.3
  8.5 0.5 collective-permute-start
  9.0 8.8 %collective-permute-done = bf16[128,2048]{1,0:T(8,128)(2,1)S(1)} collective-permute-done((bf16[128,2048]{1,0:T(8,128)(2,1)S(1)}, bf16[128,2048]{1,0:T(8,128)(2,1)S(1)}, u32[]{:S(2)}, u32[]{:S(2)}) %collective-permute-start) | collective-permute-done | bytes 524320 | tf_op jit(solution)/shard_map/ppermute | solution.py:13
  17.8 0.0 collective-permute-start.1
  17.8 8.6 %collective-permute-done.1 = bf16[128,2048]{1,0:T(8,128)(2,1)S(1)} collective-permute-done((bf16[128,2048]{1,0:T(8,128)(2,1)S(1)}, bf16[128,2048]{1,0:T(8,128)(2,1)S(1)}, u32[]{:S(2)}, u32[]{:S(2)}) %collective-permute-start.1) | collective-permute-done | bytes 524320 | tf_op jit(solution)/shard_map/ppermute | solution.py:13
  26.4 0.0 collective-permute-start.2
  26.4 8.6 %collective-permute-done.2 = bf16[128,2048]{1,0:T(8,128)(2,1)S(1)} collective-permute-done((bf16[128,2048]{1,0:T(8,128)(2,1)S(1)}, bf16[128,2048]{1,0:T(8,128)(2,1)S(1)}, u32[]{:S(2)}, u32[]{:S(2)}) %collective-permute-start.2) | collective-permute-done | bytes 524320 | tf_op jit(solution)/shard_map/ppermute | solution.py:13
  35.0 0.8 constant_dynamic-update-slice_fusion.7
  35.9 0.8 constant_dynamic-update-slice_fusion.6
  36.7 0.8 constant_dynamic-update-slice_fusion.5
  37.5 1.0 constant_dynamic-update-slice_fusion.4
  38.5 0.8 constant_dynamic-update-slice_fusion.3
  39.3 0.8 constant_dynamic-update-slice_fusion.2
  40.2 0.8 constant_dynamic-update-slice_fusion.1
  41.0 1.0 constant_dynamic-update-slice_fusion
  42.0 119.3 %all-gather.3.cloned.1.call-done = bf16[2048,2048]{1,0:T(8,128)(2,1)} async-done(((bf16[512,2048]{1,0:T(8,128)(2,1)}), bf16[2048,2048]{1,0:T(8,128)(2,1)}) %all-gather.3.cloned.1.call-update) | async-done | bytes 8388624 | tf_op jit(solution)/shard_map/all_gather | solution.py:25
  161.3 149.4 %all-gather.5.cloned.1.call-done = bf16[2048,2048]{1,0:T(8,128)(2,1)} async-done(((bf16[2048,512]{1,0:T(8,128)(2,1)}), bf16[2048,2048]{1,0:T(8,128)(2,1)}) %all-gather.5.cloned.1.call-update) | async-done | bytes 8388624 | tf_op jit(solution)/shard_map/all_gather | solution.py:29
  310.7 16.5 %convolution_convert_fusion = bf16[512,2048]{1,0:T(8,128)(2,1)} fusion(bf16[2048,2048]{1,0:T(8,128)(2,1)} %all-gather.5.cloned.1.call-done, bf16[2048,2048]{1,0:T(8,128)(2,1)} %all-gather.3.cloned.1.call-done, bf16[1024,2048]{1,0:T(8,128)(2,1)} %constant_dynamic-update-slice_fusion, s32[]{:T(128)S(6)} %select_n.14), kind=kOutput, calls=%fused_computation.1 | convolution fusion | flops 8594128896 | bytes 20971524 | tf_op jit(solution)/shard_map/dot_general | solution.py:28
  327.2 0.0 reduce-scatter.2.cloned.1.call-update
  327.2 29.5 %reduce-scatter.2.cloned.1.call-done = bf16[128,2048]{1,0:T(8,128)(2,1)} async-done(((bf16[512,2048]{1,0:T(8,128)(2,1)}), bf16[128,2048]{1,0:T(8,128)(2,1)}) %reduce-scatter.2.cloned.1.call-update) | async-done | bytes 524304 | tf_op jit(solution)/shard_map/reduce_scatter | solution.py:31
  356.7 2.0 fusion.4
  (1 shorter events, 0.0 us)
Async XLA Ops:
  6.5 1.5 copy-start
  6.5 1.7 copy-start.1
  6.5 154.7 %all-gather.3.cloned.1.call-start = ((), (), s32[]{:S(2)}) async-start(), calls=%async_computation.1 | async-start | bytes 10485760 | tf_op jit(solution)/shard_map/all_gather | solution.py:25
  7.3 303.4 %all-gather.5.cloned.1.call-start = ((), (), s32[]{:S(2)}) async-start(), calls=%async_computation.2 | async-start | bytes 10485760 | tf_op jit(solution)/shard_map/all_gather | solution.py:29
  8.0 348.7 %reduce-scatter.2.cloned.1.call-start = ((), (), s32[]{:S(2)}) async-start(), calls=%async_computation.3 | async-start | bytes 2621440 | tf_op jit(solution)/shard_map/reduce_scatter | solution.py:31
  8.5 9.3 %collective-permute-start = (bf16[128,2048]{1,0:T(8,128)(2,1)S(1)}, bf16[128,2048]{1,0:T(8,128)(2,1)S(1)}, u32[]{:S(2)}, u32[]{:S(2)}) collective-permute-start(bf16[128,2048]{1,0:T(8,128)(2,1)S(1)} %fusion.3), channel_id=1, source_target_pairs={{0,1},{1,2},{2,3},{3,0},{4,5},{5,6},{6,7},{7,4},{8,9},{9,10},{10,1... | collective-permute-start | bytes 1572872 | tf_op jit(solution)/shard_map/ppermute | solution.py:13
  17.8 8.6 %collective-permute-start.1 = (bf16[128,2048]{1,0:T(8,128)(2,1)S(1)}, bf16[128,2048]{1,0:T(8,128)(2,1)S(1)}, u32[]{:S(2)}, u32[]{:S(2)}) collective-permute-start(bf16[128,2048]{1,0:T(8,128)(2,1)S(1)} %collective-permute-done), channel_id=1, source_target_pairs={{0,1},{1,2},{2,3},{3,0},{4,5},{5,6},{6,7},{7,4},{8,9},{9,10},{10,1... | collective-permute-start | bytes 1572872 | tf_op jit(solution)/shard_map/ppermute | solution.py:13
  26.4 8.6 %collective-permute-start.2 = (bf16[128,2048]{1,0:T(8,128)(2,1)S(1)}, bf16[128,2048]{1,0:T(8,128)(2,1)S(1)}, u32[]{:S(2)}, u32[]{:S(2)}) collective-permute-start(bf16[128,2048]{1,0:T(8,128)(2,1)S(1)} %collective-permute-done.1), channel_id=1, source_target_pairs={{0,1},{1,2},{2,3},{3,0},{4,5},{5,6},{6,7},{7,4},{8,9},{9,10},{10,1... | collective-permute-start | bytes 1572872 | tf_op jit(solution)/shard_map/ppermute | solution.py:13
Sparse Core Ops, SparseCore 0:
  8.9 152.3 all-gather.2
  162.8 147.7 all-gather.4
  327.3 29.3 reduce-scatter.1
